TPU v7x, 32 devices: a whole 2x2x4 slice. The times are simulated.
32 devices in a mesh: kv: 4 (over y, x), tp: 8 (over z, core).
Axes of the slice: x: 2, y: 2, z: 4, core: 2. Of those that a mesh axis runs over, the one named last changes fastest.
Arguments:
- resid: bfloat16 [32, 4096], P('tp', 'kv'), may hold values from -35 to 35
- attn_gain: bfloat16 [4096], replicated, may hold values from 0.099609375 to 1.8984375
- w_query_nope: bfloat16 [4096, 8192], P('kv', 'tp'), may hold values from -0.09375 to 0.09375
- w_query_rope: bfloat16 [4096, 4096], P('kv', 'tp'), may hold values from -0.09375 to 0.09375
- w_latent: bfloat16 [4096, 512], P('kv'), may hold values from -0.09375 to 0.09375
- w_key_rope: bfloat16 [4096, 64], replicated, may hold values from -0.09375 to 0.09375
- latent_gain: bfloat16 [512], replicated, may hold values from 0.099609375 to 1.8984375
- key_up: bfloat16 [512, 64, 128], P(None, 'tp'), may hold values from -0.5 to 0.5
- value_up: bfloat16 [512, 64, 128], P(None, 'tp'), may hold values from -0.25 to 0.25
- w_out: bfloat16 [8192, 4096], P('tp', 'kv'), may hold values from -4 to 4
- post_gain: bfloat16 [4096], replicated, may hold values from 0.099609375 to 1.8984375
- mlp_gain: bfloat16 [4096], replicated, may hold values from 0.099609375 to 1.8984375
- w_gate: bfloat16 [4096, 11008], P('kv', 'tp'), may hold values from -3 to 3
- w_up: bfloat16 [4096, 11008], P('kv', 'tp'), may hold values from -3 to 3
- w_down: bfloat16 [11008, 4096], P('tp', 'kv'), may hold values from -0.0546875 to 0.0546875
- cache_latent: bfloat16 [32, 2048, 512], P('tp', 'kv'), may hold values from -6 to 6
- cache_rope_key: bfloat16 [32, 2048, 64], P('tp', 'kv'), may hold values from -740 to 740
Outputs:
- next_resid: bfloat16 [32, 4096], P('tp', 'kv')
- new_latent: bfloat16 [32, 512], P('tp')
- new_rope_key: bfloat16 [32, 64], P('tp')
All inputs are finite; a program needn't handle non-finite values.
Results may differ from a plain program's by a relative error of at most 0.035.
Values may be sent and summed in bfloat16 or wider, within the bound.
A program may use at most 64 MiB of HBM per device.

v0:
```python
import jax
import jax.numpy as jnp
from jax import lax
from jax.sharding import PartitionSpec as P

EPS = 1e-06
THETA = 10000.0


def rotate(vector, position):
    half_width = vector.shape[-1] // 2
    frequency = THETA ** (-jnp.arange(half_width, dtype=jnp.float32) / half_width)
    angles = jnp.asarray(position, jnp.float32) * frequency
    cos_table, sin_table = (jnp.cos(angles), jnp.sin(angles))
    lower_half, upper_half = (vector[..., :half_width], vector[..., half_width:])
    return jnp.concatenate(
        [
            lower_half * cos_table - upper_half * sin_table,
            lower_half * sin_table + upper_half * cos_table,
        ],
        axis=-1,
    )


def body(
    resid,
    attn_gain,
    w_query_nope,
    w_query_rope,
    w_latent,
    w_key_rope,
    latent_gain,
    key_up,
    value_up,
    w_out,
    post_gain,
    mlp_gain,
    w_gate,
    w_up,
    w_down,
    cache_latent,
    cache_rope_key,
):
    kv_count = lax.axis_size("kv")
    kv_index = lax.axis_index("kv")
    tp_index = lax.axis_index("tp")
    own_rows, width_dev = resid.shape
    model_width = width_dev * kv_count
    heads_dev = key_up.shape[1]
    pos_dev = cache_latent.shape[1]
    context = pos_dev * kv_count
    score_scale = (key_up.shape[2] + cache_rope_key.shape[2]) ** (-0.5)
    col_start = kv_index * width_dev
    row_start = tp_index * own_rows

    def block_of(vector):
        return lax.dynamic_slice_in_dim(vector, col_start, width_dev, 0).astype(jnp.float32)[
            None, :
        ]

    gathered = lax.all_gather(resid, "tp", axis=0, tiled=True)
    batch_rows = gathered.shape[0]
    gathered_float = gathered.astype(jnp.float32)
    normed_a = (gathered_float * block_of(attn_gain)).astype(jnp.bfloat16)
    own_normed = lax.dynamic_slice_in_dim(normed_a, row_start, own_rows, 0)
    key_rows = lax.dynamic_slice_in_dim(w_key_rope, col_start, width_dev, 0)
    q_nope_sum, q_rope_sum, latent_sum, key_sum, square_sum = (
        lax.psum(
            jnp.dot(normed_a, w_query_nope, preferred_element_type=jnp.float32).astype(
                jnp.bfloat16
            ),
            "kv",
        ).astype(jnp.float32),
        lax.psum(
            jnp.dot(normed_a, w_query_rope, preferred_element_type=jnp.float32).astype(
                jnp.bfloat16
            ),
            "kv",
        ).astype(jnp.float32),
        lax.psum(
            jnp.dot(own_normed, w_latent, preferred_element_type=jnp.float32).astype(jnp.bfloat16),
            "kv",
        ).astype(jnp.float32),
        lax.psum(
            jnp.dot(own_normed, key_rows, preferred_element_type=jnp.float32).astype(jnp.bfloat16),
            "kv",
        ).astype(jnp.float32),
        lax.psum(
            jnp.sum(gathered_float * gathered_float, axis=1).astype(jnp.bfloat16), "kv"
        ).astype(jnp.float32),
    )
    scale_in = lax.rsqrt(square_sum / model_width + EPS)[:, None]
    own_scale = lax.dynamic_slice_in_dim(scale_in, row_start, own_rows, 0)
    q_nope = (q_nope_sum * scale_in).astype(jnp.bfloat16).reshape(batch_rows, heads_dev, -1)
    q_rope = rotate((q_rope_sum * scale_in).reshape(batch_rows, heads_dev, -1), context).astype(
        jnp.bfloat16
    )
    new_latent = (
        latent_sum
        * lax.rsqrt(jnp.mean(latent_sum * latent_sum, axis=1, keepdims=True) + EPS)
        * latent_gain.astype(jnp.float32)[None, :]
    ).astype(jnp.bfloat16)
    new_rope_key = rotate(key_sum * own_scale, context).astype(jnp.bfloat16)
    q_lat = jnp.einsum("bhd,chd->bhc", q_nope, key_up, preferred_element_type=jnp.float32).astype(
        jnp.bfloat16
    )
    seq_lat, seq_rope = (
        lax.all_to_all(q_lat, "tp", split_axis=0, concat_axis=1, tiled=True),
        lax.all_to_all(q_rope, "tp", split_axis=0, concat_axis=1, tiled=True),
    )
    scores = (
        jnp.einsum("bhc,bpc->bhp", seq_lat, cache_latent, preferred_element_type=jnp.float32)
        + jnp.einsum("bhr,bpr->bhp", seq_rope, cache_rope_key, preferred_element_type=jnp.float32)
    ) * score_scale
    own_score = (
        jnp.einsum("bhc,bc->bh", seq_lat, new_latent, preferred_element_type=jnp.float32)
        + jnp.einsum("bhr,br->bh", seq_rope, new_rope_key, preferred_element_type=jnp.float32)
    ) * score_scale
    local_peak = jnp.maximum(jnp.max(scores, axis=2), own_score)
    peak = lax.pmax(local_peak, "kv")
    probs = jnp.exp(scores - peak[:, :, None])
    own_prob = jnp.exp(own_score - peak)
    totals = lax.psum(jnp.sum(probs, axis=2), "kv") + own_prob
    partial_value = jnp.einsum(
        "bhp,bpc->bhc", probs.astype(jnp.bfloat16), cache_latent, preferred_element_type=jnp.float32
    )
    summed = (
        lax.psum(partial_value.astype(jnp.bfloat16), "kv").astype(jnp.float32)
        + own_prob[:, :, None] * new_latent.astype(jnp.float32)[:, None, :]
    )
    o_lat = (summed / totals[:, :, None]).astype(jnp.bfloat16)
    head_lat = lax.all_to_all(o_lat, "tp", split_axis=1, concat_axis=0, tiled=True)
    o_heads = jnp.einsum(
        "bhc,che->bhe", head_lat, value_up, preferred_element_type=jnp.float32
    ).astype(jnp.bfloat16)
    o_flat = o_heads.reshape(batch_rows, -1)
    attended = lax.psum_scatter(
        jnp.dot(o_flat, w_out, preferred_element_type=jnp.float32).astype(jnp.bfloat16),
        "tp",
        scatter_dimension=0,
        tiled=True,
    ).astype(jnp.float32)
    post_square = lax.psum(jnp.sum(attended * attended, axis=1), "kv")
    post_part = attended * lax.rsqrt(post_square / model_width + EPS)[:, None] * block_of(post_gain)
    resid_mid = (resid.astype(jnp.float32) + post_part).astype(jnp.bfloat16)
    mid_rows = lax.all_gather(resid_mid, "tp", axis=0, tiled=True)
    mid_float = mid_rows.astype(jnp.float32)
    normed_m = (mid_float * block_of(mlp_gain)).astype(jnp.bfloat16)
    gate_part = jnp.dot(normed_m, w_gate, preferred_element_type=jnp.float32)
    up_part = jnp.dot(normed_m, w_up, preferred_element_type=jnp.float32)
    square_part = jnp.sum(mid_float * mid_float, axis=1)
    gate_sum, up_sum, mid_square = (
        lax.psum(gate_part.astype(jnp.bfloat16), "kv").astype(jnp.float32),
        lax.psum(up_part.astype(jnp.bfloat16), "kv").astype(jnp.float32),
        lax.psum(square_part.astype(jnp.bfloat16), "kv").astype(jnp.float32),
    )
    scale_mid = lax.rsqrt(mid_square / model_width + EPS)[:, None]
    hidden = (jax.nn.silu(gate_sum * scale_mid) * (up_sum * scale_mid)).astype(jnp.bfloat16)
    lowered = lax.psum_scatter(
        jnp.dot(hidden, w_down, preferred_element_type=jnp.float32).astype(jnp.bfloat16),
        "tp",
        scatter_dimension=0,
        tiled=True,
    ).astype(jnp.float32)
    next_resid = (resid_mid.astype(jnp.float32) + lowered).astype(jnp.bfloat16)
    return (next_resid, new_latent, new_rope_key)


def solution(mesh):
    return jax.shard_map(
        body,
        mesh=mesh,
        in_specs=(
            P("tp", "kv"),
            P(),
            P("kv", "tp"),
            P("kv", "tp"),
            P("kv", None),
            P(),
            P(),
            P(None, "tp", None),
            P(None, "tp", None),
            P("tp", "kv"),
            P(),
            P(),
            P("kv", "tp"),
            P("kv", "tp"),
            P("tp", "kv"),
            P("tp", "kv", None),
            P("tp", "kv", None),
        ),
        out_specs=(P("tp", "kv"), P("tp", None), P("tp", None)),
        check_vma=False,
    )
```

profile of v0, /device:TPU:0, one launch (start us, length us, event | category | flops | bytes accessed | tf_op | source)
XLA Modules:
  0.0 386.5 jit_solution(13030384441631528125)
XLA Ops:
  7.2 16.0 %all-gather = bf16[8,4,1024]{2,1,0:T(4,128)(2,1)S(1)} all-gather(bf16[1,4,1024]{2,1,0:T(4,128)(2,1)} %bitcast.69), channel_id=1, replica_groups=mesh['kv'=4,'tp'=8] {'tp'}, dimensions={0}, use_global_device_ids=true | all-gather | bytes 73728 | tf_op jit(solution)/shard_map/all_gather | solution.py:61
  23.3 0.7 dynamic-slice_convert_fusion.2
  24.0 0.1 multiply_reduce_fusion.1
  24.1 1.0 convolution_convert_fusion.10
  25.2 1.5 convolution_convert_fusion.9
  26.6 1.5 convolution_convert_fusion.8
  28.1 16.7 %all-reduce.2 = (bf16[32]{0:T(256)(128)(2,1)S(1)}, bf16[32,512]{1,0:T(8,128)(2,1)S(1)}, bf16[4,512]{1,0:T(4,128)(2,1)S(1)}, bf16[4,64]{1,0:T(4,128)(2,1)S(1)}) all-reduce(bf16[32]{0:T(256)(128)(2,1)S(1)} %get-tuple-element.15, bf16[32,512]{1,0:T(8,128)(2,1)S(1)} %convolution_convert_fusion.8, ...), channel_id=1, replica_groups=mesh['kv'=4,'tp'=8] {'kv'}, use_global_device_ids=true, to_apply=%region_2.0 | all-reduce | flops 18720 | bytes 74880 | tf_op jit(solution)/shard_map/psum | solution.py:88
  45.2 0.7 reshape.73
  46.0 4.6 %all-to-all-start.1 = ((bf16[8,2,1024]{2,1,0:T(2,128)(2,1)}), bf16[8,2,1024]{2,1,0:T(2,128)(2,1)S(1)}, u32[]{:S(2)}, u32[]{:S(2)}) async-start(bf16[8,2,1024]{2,1,0:T(2,128)(2,1)} %reshape.73), calls=%async_computation.1 | async-start | bytes 65536 | tf_op jit(solution)/shard_map/all_to_all | solution.py:109
  50.7 2.7 convolution_convert_fusion.7
  53.6 0.1 fusion.32
  53.7 42.1 %all-reduce.10.cloned.1.call-done = bf16[32,1024]{1,0:T(8,128)(2,1)} async-done(((bf16[32,1024]{1,0:T(8,128)(2,1)}), bf16[32,1024]{1,0:T(8,128)(2,1)}) %all-reduce.10.cloned.1.call-update) | async-done | bytes 65552 | tf_op jit(solution)/shard_map/psum | solution.py:68
  95.8 1.8 fusion.1
  97.6 0.9 copy.35
  98.4 4.6 %all-to-all-start = ((bf16[32,8,512]{2,1,0:T(8,128)(2,1)}), bf16[32,8,512]{2,1,0:T(8,128)(2,1)S(1)}, u32[]{:S(2)}, u32[]{:S(2)}) async-start(bf16[32,8,512]{2,1,0:T(8,128)(2,1)} %copy.35), calls=%async_computation | async-start | bytes 524288 | tf_op jit(solution)/shard_map/all_to_all | solution.py:108
  103.2 0.1 reshape.74
  103.3 0.1 fusion.23
  103.5 9.3 %all-to-all-done = bf16[32,8,512]{2,1,0:T(8,128)(2,1)S(1)} async-done(((bf16[32,8,512]{2,1,0:T(8,128)(2,1)}), bf16[32,8,512]{2,1,0:T(8,128)(2,1)S(1)}, u32[]{:S(2)}, u32[]{:S(2)}) %all-to-all-start) | async-done | bytes 262176 | tf_op jit(solution)/shard_map/all_to_all | solution.py:108
  112.7 2.3 fusion.10
  115.1 0.2 fusion.8
  115.3 1.3 fusion.48
  116.5 8.9 %pmax.7 = f32[4,64]{1,0:T(4,128)S(1)} all-reduce(f32[4,64]{1,0:T(4,128)S(1)} %fusion.39), channel_id=1, replica_groups=mesh['kv'=4,'tp'=8] {'kv'}, use_global_device_ids=true, to_apply=%region_8.0 | all-reduce | flops 256 | bytes 2048 | tf_op jit(solution)/shard_map/pmax | solution.py:120
  125.5 2.8 convolution_convert_fusion.2
  128.4 0.2 fusion.5
  128.6 8.9 %psum.83 = f32[4,64]{1,0:T(4,128)S(1)} all-reduce(f32[4,64]{1,0:T(4,128)S(1)} %fusion.5), channel_id=1, replica_groups=mesh['kv'=4,'tp'=8] {'kv'}, use_global_device_ids=true, to_apply=%region_11.0 | all-reduce | flops 256 | bytes 2048 | tf_op jit(solution)/shard_map/psum | solution.py:123
  137.5 32.0 %all-reduce.12.cloned.1.call-done = bf16[4,64,512]{2,1,0:T(8,128)(2,1)} async-done(((bf16[4,64,512]{2,1,0:T(8,128)(2,1)}), bf16[4,64,512]{2,1,0:T(8,128)(2,1)}) %all-reduce.12.cloned.1.call-update) | async-done | bytes 262160 | tf_op jit(solution)/shard_map/psum | solution.py:128
  169.5 1.1 divide_convert_fusion
  170.6 0.2 copy.38
  170.9 14.1 %all_to_all.54 = bf16[4,64,512]{2,0,1:T(4,128)(2,1)S(1)} all-to-all(bf16[4,64,512]{2,0,1:T(4,128)(2,1)S(1)} %copy.38), channel_id=1, replica_groups=mesh['kv'=4,'tp'=8] {'tp'}, dimensions={1} | all-to-all | bytes 524288 | tf_op jit(solution)/shard_map/all_to_all | solution.py:132
  185.2 1.5 fusion.2
  186.7 2.7 convolution_convert_fusion.6
  189.5 0.7 dynamic-slice_convert_fusion.1
  190.2 0.6 dynamic-slice.4
  191.4 50.8 %all-reduce.14.cloned.1.call-done = bf16[32,1024]{1,0:T(8,128)(2,1)} async-done(((bf16[32,1024]{1,0:T(8,128)(2,1)}), bf16[32,1024]{1,0:T(8,128)(2,1)}) %all-reduce.14.cloned.1.call-update) | async-done | bytes 65552
  242.2 0.8 fusion.28
  243.1 0.7 dynamic-slice_convert_fusion
  243.8 9.8 %psum.84 = f32[4]{0:T(128)S(1)} all-reduce(f32[4]{0:T(128)S(1)} %fusion.28), channel_id=1, replica_groups=mesh['kv'=4,'tp'=8] {'kv'}, use_global_device_ids=true, to_apply=%region_14.0 | all-reduce | flops 4 | bytes 32 | tf_op jit(solution)/shard_map/psum | solution.py:143
  253.6 0.8 fusion.31
  254.4 14.0 %all-gather.1 = bf16[8,4,1024]{2,1,0:T(4,128)(2,1)S(1)} all-gather(bf16[1,4,1024]{2,1,0:T(4,128)(2,1)S(1)} %bitcast.68), channel_id=1, replica_groups=mesh['kv'=4,'tp'=8] {'tp'}, dimensions={0}, use_global_device_ids=true | all-gather | bytes 73728 | tf_op jit(solution)/shard_map/all_gather | solution.py:146
  268.4 0.1 multiply_reduce_fusion
  268.5 1.6 convolution_convert_fusion.1
  270.2 1.6 convolution_convert_fusion
  271.8 8.0 %psum.86 = bf16[32]{0:T(256)(128)(2,1)S(1)} all-reduce(bf16[32]{0:T(256)(128)(2,1)S(1)} %multiply_reduce_fusion), channel_id=1, replica_groups=mesh['kv'=4,'tp'=8] {'kv'}, use_global_device_ids=true, to_apply=%region_17.0 | all-reduce | flops 32 | bytes 128 | tf_op jit(solution)/shard_map/psum | solution.py:155
  279.8 40.7 %all-reduce.18.cloned.1.call-done = (bf16[32,1376]{1,0:T(8,128)(2,1)}, bf16[32,1376]{1,0:T(8,128)(2,1)}) async-done(((bf16[32,1376]{1,0:T(8,128)(2,1)}, bf16[32,1376]{1,0:T(8,128)(2,1)}), (bf16[32,1376]{1,0:T(8,128)(2,1)}, bf16[32,1376]{1,0:T(8,128)(2,1)})) %all-reduce.18.cloned.1.call-update) | async-done | bytes 176144 | tf_op jit(solution)/shard_map/psum | solution.py:154
  320.5 3.2 convolution_convert_fusion.5
  323.7 0.6 pad_maximum_fusion.1
  324.4 54.3 %all-reduce.16.cloned.1.call-done = bf16[32,1024]{1,0:T(8,128)(2,1)} async-done(((bf16[32,1024]{1,0:T(8,128)(2,1)}), bf16[32,1024]{1,0:T(8,128)(2,1)}) %all-reduce.16.cloned.1.call-update) | async-done | bytes 65552
  378.6 1.3 add_convert_fusion.1
  (44 shorter events, 1.4 us)
Async XLA Ops:
  7.2 261.3 %copy-start = (bf16[1024,1376]{0,1:T(8,128)(2,1)S(1)}, bf16[1024,1376]{0,1:T(8,128)(2,1)}, u32[]{:S(2)}) copy-start(bf16[1024,1376]{0,1:T(8,128)(2,1)} %param.29) | copy-start | bytes 8454148
  46.0 52.5 %all-to-all-start.1 = ((bf16[8,2,1024]{2,1,0:T(2,128)(2,1)}), bf16[8,2,1024]{2,1,0:T(2,128)(2,1)S(1)}, u32[]{:S(2)}, u32[]{:S(2)}) async-start(bf16[8,2,1024]{2,1,0:T(2,128)(2,1)} %reshape.73), calls=%async_computation.1 | async-start | bytes 65536 | tf_op jit(solution)/shard_map/all_to_all | solution.py:109
  50.6 52.6 %copy-start.4 = (bf16[512]{0:T(512)(128)(2,1)S(1)}, bf16[512]{0:T(512)(128)(2,1)}, u32[]{:S(2)}) copy-start(bf16[512]{0:T(512)(128)(2,1)} %param.23) | copy-start | bytes 3076
  50.6 45.2 %all-reduce.10.cloned.1.call-start = ((), (), s32[]{:S(2)}) async-start(), calls=%async_computation.3 | async-start | bytes 131072 | tf_op jit(solution)/shard_map/psum | solution.py:68
  98.4 14.3 %all-to-all-start = ((bf16[32,8,512]{2,1,0:T(8,128)(2,1)}), bf16[32,8,512]{2,1,0:T(8,128)(2,1)S(1)}, u32[]{:S(2)}, u32[]{:S(2)}) async-start(bf16[32,8,512]{2,1,0:T(8,128)(2,1)} %copy.35), calls=%async_computation | async-start | bytes 524288 | tf_op jit(solution)/shard_map/all_to_all | solution.py:108
  103.0 66.5 %all-reduce.12.cloned.1.call-start = ((), (), s32[]{:S(2)}) async-start(), calls=%async_computation.4 | async-start | bytes 524288 | tf_op jit(solution)/shard_map/psum | solution.py:128
  103.2 13.3 %copy-start.3 = (bf16[4,512]{1,0:T(4,128)(2,1)}, bf16[4,512]{1,0:T(4,128)(2,1)S(1)}, u32[]{:S(2)}) copy-start(bf16[4,512]{1,0:T(4,128)(2,1)S(1)} %get-tuple-element.10) | copy-start | bytes 12292
  128.3 113.9 %all-reduce.14.cloned.1.call-start = ((), (), s32[]{:S(2)}) async-start(), calls=%async_computation.5 | async-start | bytes 131072
  185.1 5.1 %copy-start.5 = (u32[32]{0:T(128)S(1)}, u32[32]{0:T(128)}, u32[]{:S(2)}) copy-start(u32[32]{0:T(128)} %constant.53) | copy-start | bytes 388
  185.1 68.5 %copy-start.2 = (bf16[4,1024]{1,0:T(4,128)(2,1)S(1)}, bf16[4,1024]{1,0:T(4,128)(2,1)}, u32[]{:S(2)}) copy-start(bf16[4,1024]{1,0:T(4,128)(2,1)} %param.17) | copy-start | bytes 24580
  189.4 131.1 %all-reduce.18.cloned.1.call-start = ((), (), s32[]{:S(2)}) async-start(), calls=%async_computation.7 | async-start | bytes 360448 | tf_op jit(solution)/shard_map/psum | solution.py:154
  268.4 1.8 copy-start.1
  279.7 98.9 %all-reduce.16.cloned.1.call-start = ((), (), s32[]{:S(2)}) async-start(), calls=%async_computation.6 | async-start | bytes 131072
Sparse Core Ops, SparseCore 0:
  54.3 41.4 all-reduce.9
  128.4 41.0 all-reduce.11
  189.5 52.6 all-reduce.13
  279.9 40.6 all-reduce.17
  323.9 54.7 all-reduce.15
where the time goes:
time: 388 us; the launch traced here: 386 us
  waiting for transfers between devices  229 us (59%)
  blocking collectives  96.5 us (25%)
  matrix products  25.8 us (7%)
  between operations  14.6 us (4%)
  starting transfers between devices  9.46 us (2%)
  other arithmetic  8.04 us (2%)
    unnamed x7, waiting for transfers between devices  105 us
    psum x1, waiting for transfers between devices, body(): lax.psum(jnp.dot(normed_a, w_query_nope, preferred_element_type=jnp.float...  42.1 us
    psum x1, waiting for transfers between devices, body(): lax.psum(up_part.astype(jnp.bfloat16), 'kv').astype(jnp.float32)  40.7 us
    psum x1, waiting for transfers between devices, body(): lax.psum(partial_value.astype(jnp.bfloat16), 'kv').astype(jnp.float32)  32 us
    psum x1, blocking collectives, body(): lax.psum(jnp.sum(gathered_float * gathered_float, axis=1).astype(jnp.bflo...  16.7 us
    all_gather x1, blocking collectives, body(): gathered = lax.all_gather(resid, 'tp', axis=0, tiled=True)  16 us
    all_to_all x1, blocking collectives, body(): lax.all_to_all(o_lat, 'tp', split_axis=1, concat_axis=0, tiled=True)  14.1 us
    all_gather x1, blocking collectives, body(): mid_rows = lax.all_gather(resid_mid, 'tp', axis=0, tiled=True)  14 us
  transfers between devices with their start and end apart: 7, of which 6 were waited for; matrix products, arithmetic and copies ran while one was open for 2% of the time, Pallas kernels for 0%

commit v1 on v0

--- a/solution.py
+++ b/solution.py
@@ -125,7 +125,9 @@
         "bhp,bpc->bhc", probs.astype(jnp.bfloat16), cache_latent, preferred_element_type=jnp.float32
     )
     summed = (
-        lax.psum(partial_value.astype(jnp.bfloat16), "kv").astype(jnp.float32)
+        jnp.sum(lax.all_gather(partial_value.astype(jnp.bfloat16), "kv"), axis=0).astype(
+            jnp.float32
+        )
         + own_prob[:, :, None] * new_latent.astype(jnp.float32)[:, None, :]
     )
     o_lat = (summed / totals[:, :, None]).astype(jnp.bfloat16)

time: 388 us -> 372 us (0.959)
  waiting for transfers between devices: 229 us -> 213 us
    psum x1 -> x0, waiting for transfers between devices: 32 us -> none  [body(): lax.psum(partial_value.astype(jnp.bfloat16), 'kv').astype(jnp.float32)]
    all_gather x0 -> x1, waiting for transfers between devices: none -> 15.4 us  [body(): lax.all_gather(partial_value.astype(jnp.bfloat16), 'kv')]
where the time goes in v1:
time: 372 us; the launch traced here: 371 us
  waiting for transfers between devices  213 us (57%)
  blocking collectives  96.5 us (26%)
  matrix products  25.8 us (7%)
  between operations  14.6 us (4%)
  starting transfers between devices  9.46 us (3%)
  other arithmetic  8.51 us (2%)
    unnamed x7, waiting for transfers between devices  105 us
    psum x1, waiting for transfers between devices, body(): lax.psum(jnp.dot(normed_a, w_query_nope, preferred_element_type=jnp.float...  42.1 us
    psum x1, waiting for transfers between devices, body(): lax.psum(up_part.astype(jnp.bfloat16), 'kv').astype(jnp.float32)  40.7 us
    psum x1, blocking collectives, body(): lax.psum(jnp.sum(gathered_float * gathered_float, axis=1).astype(jnp.bflo...  16.7 us
    all_gather x1, blocking collectives, body(): gathered = lax.all_gather(resid, 'tp', axis=0, tiled=True)  16 us
    all_gather x1, waiting for transfers between devices, body(): lax.all_gather(partial_value.astype(jnp.bfloat16), 'kv')  15.4 us
    all_to_all x1, blocking collectives, body(): lax.all_to_all(o_lat, 'tp', split_axis=1, concat_axis=0, tiled=True)  14.1 us
    all_gather x1, blocking collectives, body(): mid_rows = lax.all_gather(resid_mid, 'tp', axis=0, tiled=True)  14 us
  transfers between devices with their start and end apart: 7, of which 6 were waited for; matrix products, arithmetic and copies ran while one was open for 2% of the time, Pallas kernels for 0%

profile of v1, /device:TPU:0, one launch (start us, length us, event | category | flops | bytes accessed | tf_op | source)
XLA Modules:
  0.0 370.6 jit_solution(6707170506068403217)
XLA Ops:
  7.2 16.0 %all-gather.1 = bf16[8,4,1024]{2,1,0:T(4,128)(2,1)S(1)} all-gather(bf16[1,4,1024]{2,1,0:T(4,128)(2,1)} %bitcast.71), channel_id=1, replica_groups=mesh['kv'=4,'tp'=8] {'tp'}, dimensions={0}, use_global_device_ids=true | all-gather | bytes 73728 | tf_op jit(solution)/shard_map/all_gather | solution.py:61
  23.3 0.7 dynamic-slice_convert_fusion.2
  24.0 0.1 multiply_reduce_fusion.1
  24.1 1.0 convolution_convert_fusion.10
  25.2 1.5 convolution_convert_fusion.9
  26.6 1.5 convolution_convert_fusion.8
  28.1 16.7 %all-reduce.2 = (bf16[32]{0:T(256)(128)(2,1)S(1)}, bf16[32,512]{1,0:T(8,128)(2,1)S(1)}, bf16[4,512]{1,0:T(4,128)(2,1)S(1)}, bf16[4,64]{1,0:T(4,128)(2,1)S(1)}) all-reduce(bf16[32]{0:T(256)(128)(2,1)S(1)} %get-tuple-element.15, bf16[32,512]{1,0:T(8,128)(2,1)S(1)} %convolution_convert_fusion.8, ...), channel_id=1, replica_groups=mesh['kv'=4,'tp'=8] {'kv'}, use_global_device_ids=true, to_apply=%region_2.0 | all-reduce | flops 18720 | bytes 74880 | tf_op jit(solution)/shard_map/psum | solution.py:88
  45.2 0.7 reshape.74
  46.0 4.6 %all-to-all-start.1 = ((bf16[8,2,1024]{2,1,0:T(2,128)(2,1)}), bf16[8,2,1024]{2,1,0:T(2,128)(2,1)S(1)}, u32[]{:S(2)}, u32[]{:S(2)}) async-start(bf16[8,2,1024]{2,1,0:T(2,128)(2,1)} %reshape.74), calls=%async_computation.1 | async-start | bytes 65536 | tf_op jit(solution)/shard_map/all_to_all | solution.py:109
  50.7 2.7 convolution_convert_fusion.7
  53.7 42.1 %all-reduce.9.cloned.1.call-done = bf16[32,1024]{1,0:T(8,128)(2,1)} async-done(((bf16[32,1024]{1,0:T(8,128)(2,1)}), bf16[32,1024]{1,0:T(8,128)(2,1)}) %all-reduce.9.cloned.1.call-update) | async-done | bytes 65552 | tf_op jit(solution)/shard_map/psum | solution.py:68
  95.8 1.8 fusion.1
  97.6 0.9 copy.45
  98.4 4.6 %all-to-all-start = ((bf16[32,8,512]{2,1,0:T(8,128)(2,1)}), bf16[32,8,512]{2,1,0:T(8,128)(2,1)S(1)}, u32[]{:S(2)}, u32[]{:S(2)}) async-start(bf16[32,8,512]{2,1,0:T(8,128)(2,1)} %copy.45), calls=%async_computation | async-start | bytes 524288 | tf_op jit(solution)/shard_map/all_to_all | solution.py:108
  103.3 0.1 fusion.23
  103.5 9.3 %all-to-all-done = bf16[32,8,512]{2,1,0:T(8,128)(2,1)S(1)} async-done(((bf16[32,8,512]{2,1,0:T(8,128)(2,1)}), bf16[32,8,512]{2,1,0:T(8,128)(2,1)S(1)}, u32[]{:S(2)}, u32[]{:S(2)}) %all-to-all-start) | async-done | bytes 262176 | tf_op jit(solution)/shard_map/all_to_all | solution.py:108
  112.7 2.3 fusion.10
  115.1 0.2 fusion.8
  115.3 1.3 fusion.48
  116.5 8.9 %pmax.7 = f32[4,64]{1,0:T(4,128)S(1)} all-reduce(f32[4,64]{1,0:T(4,128)S(1)} %fusion.39), channel_id=1, replica_groups=mesh['kv'=4,'tp'=8] {'kv'}, use_global_device_ids=true, to_apply=%region_8.0 | all-reduce | flops 256 | bytes 2048 | tf_op jit(solution)/shard_map/pmax | solution.py:120
  125.5 2.8 convolution_convert_fusion.2
  128.4 0.2 fusion.5
  128.6 8.9 %psum.75 = f32[4,64]{1,0:T(4,128)S(1)} all-reduce(f32[4,64]{1,0:T(4,128)S(1)} %fusion.5), channel_id=1, replica_groups=mesh['kv'=4,'tp'=8] {'kv'}, use_global_device_ids=true, to_apply=%region_11.0 | all-reduce | flops 256 | bytes 2048 | tf_op jit(solution)/shard_map/psum | solution.py:123
  137.5 15.4 %all-gather.5.cloned.1.call-done = bf16[16,64,512]{2,1,0:T(8,128)(2,1)} async-done(((bf16[4,64,512]{2,1,0:T(8,128)(2,1)}), bf16[16,64,512]{2,1,0:T(8,128)(2,1)}) %all-gather.5.cloned.1.call-update) | async-done | bytes 1048592 | tf_op jit(solution)/shard_map/all_gather | solution.py:128
  152.9 1.4 reduce_sum.59
  154.4 0.2 divide_convert_fusion
  154.5 0.2 copy.48
  154.7 14.1 %all_to_all.54 = bf16[4,64,512]{2,0,1:T(4,128)(2,1)S(1)} all-to-all(bf16[4,64,512]{2,0,1:T(4,128)(2,1)S(1)} %copy.48), channel_id=1, replica_groups=mesh['kv'=4,'tp'=8] {'tp'}, dimensions={1} | all-to-all | bytes 524288 | tf_op jit(solution)/shard_map/all_to_all | solution.py:134
  168.9 0.2 copy.50
  169.2 1.5 fusion.2
  170.8 2.7 convolution_convert_fusion.6
  173.5 0.7 dynamic-slice_convert_fusion.1
  174.2 0.6 dynamic-slice.4
  175.5 50.9 %all-reduce.11.cloned.1.call-done = bf16[32,1024]{1,0:T(8,128)(2,1)} async-done(((bf16[32,1024]{1,0:T(8,128)(2,1)}), bf16[32,1024]{1,0:T(8,128)(2,1)}) %all-reduce.11.cloned.1.call-update) | async-done | bytes 65552
  226.4 0.8 fusion.28
  227.2 0.7 dynamic-slice_convert_fusion
  227.9 9.8 %psum.76 = f32[4]{0:T(128)S(1)} all-reduce(f32[4]{0:T(128)S(1)} %fusion.28), channel_id=1, replica_groups=mesh['kv'=4,'tp'=8] {'kv'}, use_global_device_ids=true, to_apply=%region_14.0 | all-reduce | flops 4 | bytes 32 | tf_op jit(solution)/shard_map/psum | solution.py:145
  237.7 0.8 fusion.31
  238.5 14.0 %all-gather.2 = bf16[8,4,1024]{2,1,0:T(4,128)(2,1)S(1)} all-gather(bf16[1,4,1024]{2,1,0:T(4,128)(2,1)S(1)} %bitcast.70), channel_id=1, replica_groups=mesh['kv'=4,'tp'=8] {'tp'}, dimensions={0}, use_global_device_ids=true | all-gather | bytes 73728 | tf_op jit(solution)/shard_map/all_gather | solution.py:148
  252.5 0.1 multiply_reduce_fusion
  252.6 1.6 convolution_convert_fusion.1
  254.3 1.6 convolution_convert_fusion
  255.9 8.0 %psum.78 = bf16[32]{0:T(256)(128)(2,1)S(1)} all-reduce(bf16[32]{0:T(256)(128)(2,1)S(1)} %multiply_reduce_fusion), channel_id=1, replica_groups=mesh['kv'=4,'tp'=8] {'kv'}, use_global_device_ids=true, to_apply=%region_17.0 | all-reduce | flops 32 | bytes 128 | tf_op jit(solution)/shard_map/psum | solution.py:157
  263.9 40.7 %all-reduce.15.cloned.1.call-done = (bf16[32,1376]{1,0:T(8,128)(2,1)}, bf16[32,1376]{1,0:T(8,128)(2,1)}) async-done(((bf16[32,1376]{1,0:T(8,128)(2,1)}, bf16[32,1376]{1,0:T(8,128)(2,1)}), (bf16[32,1376]{1,0:T(8,128)(2,1)}, bf16[32,1376]{1,0:T(8,128)(2,1)})) %all-reduce.15.cloned.1.call-update) | async-done | bytes 176144 | tf_op jit(solution)/shard_map/psum | solution.py:156
  304.7 3.2 convolution_convert_fusion.5
  307.9 0.6 pad_maximum_fusion.1
  308.5 54.3 %all-reduce.13.cloned.1.call-done = bf16[32,1024]{1,0:T(8,128)(2,1)} async-done(((bf16[32,1024]{1,0:T(8,128)(2,1)}), bf16[32,1024]{1,0:T(8,128)(2,1)}) %all-reduce.13.cloned.1.call-update) | async-done | bytes 65552
  362.8 1.3 add_convert_fusion.1
  (46 shorter events, 1.6 us)
Async XLA Ops:
  7.2 245.5 %copy-start = (bf16[1024,1376]{0,1:T(8,128)(2,1)S(1)}, bf16[1024,1376]{0,1:T(8,128)(2,1)}, u32[]{:S(2)}) copy-start(bf16[1024,1376]{0,1:T(8,128)(2,1)} %param.29) | copy-start | bytes 8454148
  46.0 52.5 %all-to-all-start.1 = ((bf16[8,2,1024]{2,1,0:T(2,128)(2,1)}), bf16[8,2,1024]{2,1,0:T(2,128)(2,1)S(1)}, u32[]{:S(2)}, u32[]{:S(2)}) async-start(bf16[8,2,1024]{2,1,0:T(2,128)(2,1)} %reshape.74), calls=%async_computation.1 | async-start | bytes 65536 | tf_op jit(solution)/shard_map/all_to_all | solution.py:109
  50.6 52.6 %copy-start.4 = (bf16[512]{0:T(512)(128)(2,1)S(1)}, bf16[512]{0:T(512)(128)(2,1)}, u32[]{:S(2)}) copy-start(bf16[512]{0:T(512)(128)(2,1)} %param.23) | copy-start | bytes 3076
  50.6 45.2 %all-reduce.9.cloned.1.call-start = ((), (), s32[]{:S(2)}) async-start(), calls=%async_computation.3 | async-start | bytes 131072 | tf_op jit(solution)/shard_map/psum | solution.py:68
  98.4 14.3 %all-to-all-start = ((bf16[32,8,512]{2,1,0:T(8,128)(2,1)}), bf16[32,8,512]{2,1,0:T(8,128)(2,1)S(1)}, u32[]{:S(2)}, u32[]{:S(2)}) async-start(bf16[32,8,512]{2,1,0:T(8,128)(2,1)} %copy.45), calls=%async_computation | async-start | bytes 524288 | tf_op jit(solution)/shard_map/all_to_all | solution.py:108
  103.0 49.9 %all-gather.5.cloned.1.call-start = ((), (), s32[]{:S(2)}) async-start(), calls=%async_computation.4 | async-start | bytes 1310720 | tf_op jit(solution)/shard_map/all_gather | solution.py:128
  103.2 13.3 %copy-start.3 = (bf16[4,512]{1,0:T(4,128)(2,1)}, bf16[4,512]{1,0:T(4,128)(2,1)S(1)}, u32[]{:S(2)}) copy-start(bf16[4,512]{1,0:T(4,128)(2,1)S(1)} %get-tuple-element.10) | copy-start | bytes 12292
  128.3 98.0 %all-reduce.11.cloned.1.call-start = ((), (), s32[]{:S(2)}) async-start(), calls=%async_computation.5 | async-start | bytes 131072
  169.1 5.1 %copy-start.5 = (u32[32]{0:T(128)S(1)}, u32[32]{0:T(128)}, u32[]{:S(2)}) copy-start(u32[32]{0:T(128)} %constant.55) | copy-start | bytes 388
  169.1 68.6 %copy-start.2 = (bf16[4,1024]{1,0:T(4,128)(2,1)S(1)}, bf16[4,1024]{1,0:T(4,128)(2,1)}, u32[]{:S(2)}) copy-start(bf16[4,1024]{1,0:T(4,128)(2,1)} %param.17) | copy-start | bytes 24580
  173.5 131.2 %all-reduce.15.cloned.1.call-start = ((), (), s32[]{:S(2)}) async-start(), calls=%async_computation.7 | async-start | bytes 360448 | tf_op jit(solution)/shard_map/psum | solution.py:156
  252.5 1.8 copy-start.1
  263.9 98.9 %all-reduce.13.cloned.1.call-start = ((), (), s32[]{:S(2)}) async-start(), calls=%async_computation.6 | async-start | bytes 131072
Sparse Core Ops, SparseCore 0:
  54.3 41.4 all-reduce.8
  128.4 24.4 all-gather.4
  173.6 52.7 all-reduce.10
  264.0 40.6 all-reduce.14
  308.0 54.7 all-reduce.12
